TPU v7x, 32 devices: a whole 2x2x4 slice. The times are simulated.
32 devices in a mesh: ep: 4 (over z), tp: 8 (over y, x, core).
Axes of the slice: x: 2, y: 2, z: 4, core: 2. Of those that a mesh axis runs over, the one named last changes fastest.
Arguments:
- queries: bfloat16 [1024, 2048], P('ep', 'tp'), may hold values from -6 to 6
- key_rows: bfloat16 [1024, 1024], P('ep', 'tp'), may hold values from -6 to 6
- values: bfloat16 [1024, 1024], P('ep', 'tp'), may hold values from -140 to 140
- query_gain: float32 [64], replicated, may hold values from 0.55 to 7.5
- key_gain: float32 [64], replicated, may hold values from 0.55 to 7.5
- mix_gain: float32 [2048], replicated, may hold values from 0.1 to 1.9
- out_weight: bfloat16 [2048, 4096], P(None, 'tp'), may hold values from -0.125 to 0.125
- expert_input: bfloat16 [1024, 4096], P('ep', 'tp'), may hold values from -140 to 140
- expert_gain: float32 [4096], replicated, may hold values from 0.1 to 1.9
- route_ids: int32 [1024, 2], P('ep'), may hold values from 0 to 3, as said below
- route_weights: float32 [1024, 2], P('ep'), may hold values from 0.3 to 1.7
- expert_gate: bfloat16 [4, 4096, 2048], P('ep', None, 'tp'), may hold values from -0.09375 to 0.09375
- expert_up: bfloat16 [4, 4096, 2048], P('ep', None, 'tp'), may hold values from -0.09375 to 0.09375
- expert_down: bfloat16 [4, 2048, 4096], P('ep', None, 'tp'), may hold values from -0.125 to 0.125
Outputs:
- attended: bfloat16 [1024, 4096], P('ep', 'tp')
- expert_mix: bfloat16 [1024, 4096], P('ep', 'tp')
Inputs may be any that keep to these rules, and one draw needn't show every extreme that they name: `route_ids`: the 2 experts of a row differ. In every aligned block of 256 rows no expert is named more than 171 times, and one expert, the same for all blocks, is named exactly 171 times in every block.
All inputs are finite; a program needn't handle non-finite values.
Results may differ from a plain program's by a relative error of at most 0.01.
The roundings to bfloat16 on the way count: a program that leaves them out, or rounds other values in their place, can miss the bound.
Values may be sent and summed in bfloat16 or wider, within the bound.
A program may use at most 64 MiB of HBM per device.

v0:
```python
import functools
import math

import jax
import jax.numpy as jnp
import numpy as np
from jax import lax
from jax.experimental import pallas as pl
from jax.experimental.pallas import tpu as pltpu
from jax.sharding import PartitionSpec as P

Q_HEADS = 32
KV_HEADS = 16
HEAD = 64
GRID_W = 64
EPS = 1e-06
THETA = 10000.0
MESH = pl.DeviceIdType.MESH
F32 = jnp.float32
BF16 = jnp.bfloat16


def gather_plan(n_tp):
    if n_tp == 8:
        return (
            (2, 0, None, None),
            (4, 0, None, None),
            (1, 0, None, None),
            (4, 2, 0, 0),
            (2, 4, 1, 1),
            (1, 2, None, 0),
            (1, 4, None, 1),
            (1, 6, 0, 3),
            (1, 6, 1, 4),
        )
    return tuple((m, 0, None, None) for m in range(1, n_tp))


def plan_stages(plan):
    depth = []
    for entry in plan:
        depth.append(0 if entry[3] is None else depth[entry[3]] + 1)
    return [[i for i, d in enumerate(depth) if d == k] for k in range(3)]


class Gather:
    def __init__(self, name, plan, buf, send, recv, tp):
        self.name = name
        self.plan, self.buf, self.send, self.recv, self.tp = plan, buf, send, recv, tp
        self.stages = plan_stages(plan)
        self.waited = set()
        self.sent = []

    def part(self, block, half):
        if half is None:
            return self.buf.at[block]
        width = self.buf.shape[-1] // 2
        return self.buf.at[block, :, pl.ds(half * width, width)]

    def copy(self, i):
        target, block, half, _ = self.plan[i]
        return pltpu.make_async_remote_copy(
            src_ref=self.part(block, half),
            dst_ref=self.part(block ^ target, half),
            send_sem=self.send.at[i],
            recv_sem=self.recv.at[i],
            device_id={"tp": self.tp ^ target},
            device_id_type=MESH,
        )

    def wait_entry(self, i):
        if i not in self.waited:
            self.waited.add(i)
            with jax.named_scope(f"w{self.name}_{i}"):
                self.copy(i).wait_recv()

    def stage(self, k):
        for i in self.stages[k]:
            if self.plan[i][3] is not None:
                self.wait_entry(self.plan[i][3])
            copy = self.copy(i)
            copy.start()
            self.sent.append(copy)

    def ready(self, block):
        for i, entry in enumerate(self.plan):
            if entry[1] ^ entry[0] == block:
                self.wait_entry(i)

    def order(self):
        blocks = [0]
        for entry in self.plan:
            if entry[0] ^ entry[1] not in blocks:
                blocks.append(entry[0] ^ entry[1])
        return blocks

    def drain(self):
        for copy in self.sent:
            copy.wait_send()


def iota(shape, axis):
    return lax.broadcasted_iota(jnp.int32, shape, axis)


def exact_dot(a, b):
    return jnp.dot(a, b, precision=lax.Precision.HIGHEST, preferred_element_type=F32)


def norm_turn(source, gain, cosine, sine):
    width = source.shape[1]
    rows = source.astype(F32)
    i0, i1 = iota((width, width), 0), iota((width, width), 1)
    same_head = jnp.where(i0 // HEAD == i1 // HEAD, 1.0 / HEAD, 0.0).astype(F32)
    mean = exact_dot(rows * rows, same_head)
    rows = rows * lax.rsqrt(mean + EPS) * gain
    partner = jnp.where(i1 % 2 == 0, i1 + 1, i1 - 1)
    sign = jnp.where(i1 % 2 == 0, -1.0, 1.0)
    swap = jnp.where(i0 == partner, sign, 0.0).astype(F32)
    return rows * cosine + exact_dot(rows, swap) * sine


def tables(cos_ref, sin_ref, offset):
    length, width = cos_ref.shape
    half_width = HEAD // 2
    inverse = THETA ** (-np.arange(0, half_width, 2, dtype=np.float32) / half_width)
    pair = iota((1, width), 1) % HEAD // 2
    row_inv = jnp.zeros((1, width), F32)
    for m, value in enumerate(inverse.astype(np.float32)):
        row_inv = jnp.where(pair % len(inverse) == m, float(value), row_inv)
    position = offset + iota((length, width), 0)
    grid = jnp.where(
        iota((length, width), 1) % HEAD < half_width, position // GRID_W, position % GRID_W
    ).astype(F32)
    angle = grid * row_inv
    cos_ref[...] = jnp.cos(angle)
    sin_ref[...] = jnp.sin(angle)


def kernel(
    n_ep, n_tp, cap, plan,
    q_ref, k_ref, v_ref, qg_ref, kg_ref, mg_ref, wo_hbm, x_ref, xg_ref,
    idst_ref, rwt_ref, wg_hbm, wu_hbm, wd_hbm,
    att_ref, mix_ref,
    cos_ref, sin_ref, xo, xb, hb, mb, kb, vb, qb, ob, rb, wgu, wd, wo,
    w_sem, v_sem,
    xz_send, xz_recv, kz_send, kz_recv, vz_send, vz_recv, rz_send, rz_recv,
    xt_send, xt_recv, ht_send, ht_recv, mt_send, mt_recv,
):
    ep, tp = lax.axis_index("ep"), lax.axis_index("tp")
    groups = xb.shape[0]
    per = n_ep // groups
    length = x_ref.shape[0]
    ffw = hb.shape[-1]

    barrier = pltpu.get_barrier_semaphore()
    for d in range(1, n_ep):
        pl.semaphore_signal(barrier, inc=1, device_id={"ep": ep ^ d}, device_id_type=MESH)
    for m in range(1, n_tp):
        pl.semaphore_signal(barrier, inc=1, device_id={"tp": tp ^ m}, device_id_type=MESH)

    lanes = (n_ep + 15) // 16 * 16
    hit_t = [(idst_ref[k : k + 1, :] == iota((lanes, length), 0)) for k in range(2)]
    both_t = sum(jnp.where(h, 1.0, 0.0) for h in hit_t).astype(BF16)
    i0, i1 = iota((length, length), 0), iota((length, length), 1)
    before_t = jnp.where(i0 < i1, 1.0, 0.0).astype(BF16)
    count_t = jnp.dot(both_t, before_t, preferred_element_type=F32)
    slot_t = [
        jnp.sum(jnp.where(hit_t[k], count_t, 0.0), axis=0, keepdims=True).astype(jnp.int32)
        + idst_ref[k : k + 1, :] * cap
        for k in range(2)
    ]

    def picked_rows(d):
        index = (ep ^ d) * cap + iota((cap, length), 0)
        choose = jnp.where((slot_t[0] == index) | (slot_t[1] == index), 1.0, 0.0).astype(BF16)
        return jnp.dot(choose, x_ref[...], preferred_element_type=F32).astype(BF16)

    sends = []

    def ep_copy(source, target, d, send, recv):
        return pltpu.make_async_remote_copy(
            src_ref=source, dst_ref=target, send_sem=send.at[d], recv_sem=recv.at[d],
            device_id={"ep": ep ^ d}, device_id_type=MESH,
        )

    def x_copy(d):
        return ep_copy(
            xo.at[d], xb.at[d // per, 0, pl.ds((d % per) * cap, cap)], d, xz_send, xz_recv
        )

    xt = [Gather(f"x{c}", plan, xb.at[c], xt_send.at[c], xt_recv.at[c], tp) for c in range(groups)]
    ht = [Gather(f"h{c}", plan, hb.at[c], ht_send.at[c], ht_recv.at[c], tp) for c in range(groups)]
    mt = Gather("m", plan, mb, mt_send, mt_recv, tp)

    xb[0, 0, pl.ds(0, cap), :] = picked_rows(0)
    pl.semaphore_wait(barrier, n_ep + n_tp - 2)
    if per == 1:
        xt[0].stage(0)

    def send_rows(c):
        for d in range(c * per, (c + 1) * per):
            if d:
                copy = x_copy(d)
                copy.start()
                sends.append(copy)

    for d in range(1, n_ep):
        xo[d] = picked_rows(d)
        if d == max(per - 1, 1):
            for c in range(0 if per > 1 else 1, 1 if per > 1 else 2):
                send_rows(c)

    def x_first(c):
        for d in range(c * per, (c + 1) * per):
            if d:
                x_copy(d).wait_recv()
        xt[c].stage(0)

    local = []
    for m in range(n_tp):
        p = tp ^ m
        pieces = (
            (wg_hbm.at[p], wgu.at[m, :, pl.ds(0, ffw)]),
            (wu_hbm.at[p], wgu.at[m, :, pl.ds(ffw, ffw)]),
            (wd_hbm.at[p], wd.at[m]),
            (wo_hbm.at[p], wo.at[m]),
        )
        for k, (source, target) in enumerate(pieces):
            copy = pltpu.make_async_copy(source, target, w_sem.at[k, m])
            copy.start()
            local.append(((k, m), copy))
    local = dict(local)
    own_v = pltpu.make_async_copy(v_ref, vb.at[0], v_sem.at[0])
    own_v.start()

    if per > 1:
        x_first(0)

    tables(cos_ref, sin_ref, ep * length)
    kb[0] = norm_turn(
        k_ref[...],
        jnp.concatenate([kg_ref[...]] * (k_ref.shape[1] // HEAD), axis=1),
        cos_ref[:, : k_ref.shape[1]],
        sin_ref[:, : k_ref.shape[1]],
    ).astype(BF16)
    own_v.wait()

    def send_keys():
        for d in range(1, n_ep):
            for source, target, send, recv in (
                (kb.at[0], kb.at[d], kz_send, kz_recv),
                (vb.at[0], vb.at[d], vz_send, vz_recv),
            ):
                copy = ep_copy(source, target, d, send, recv)
                copy.start()
                sends.append(copy)

    def turn_queries():
        qw = cos_ref.shape[1]
        gain = jnp.concatenate([qg_ref[...]] * (qw // HEAD), axis=1)
        for i in range(q_ref.shape[1] // qw):
            part = pl.ds(i * qw, qw)
            turned = norm_turn(q_ref[:, part], gain, cos_ref[...], sin_ref[...])
            qb[:, part] = (turned.astype(BF16).astype(F32) * (1.0 / math.sqrt(HEAD))).astype(BF16)

    fetched = set()

    def weights(k, m):
        if (k, m) not in fetched:
            fetched.add((k, m))
            local[k, m].wait()

    def hidden(c):
        rows = xb.shape[2]
        total = jnp.zeros((rows, 2 * ffw), F32)
        squares = jnp.zeros((rows, 1), F32)
        for m in xt[c].order():
            xt[c].ready(m)
            weights(0, m)
            weights(1, m)
            block = xb[c, m].astype(F32)
            squares += jnp.sum(block * block, axis=1, keepdims=True)
            scaled = (block * xg_ref[tp ^ m]).astype(BF16)
            total += jnp.dot(scaled, wgu[m], preferred_element_type=F32)
        stat = lax.rsqrt(squares / xg_ref.shape[0] / xg_ref.shape[2] + EPS)
        gate = total[:, :ffw] * stat
        up = total[:, ffw:] * stat
        hb[c, 0] = (gate / (1.0 + jnp.exp(-gate)) * up).astype(BF16)

    def r_copy(d):
        return ep_copy(
            ob.at[d // per, pl.ds((d % per) * cap, cap)], rb.at[d], d, rz_send, rz_recv
        )

    def down(c):
        total = jnp.zeros((ob.shape[1], ob.shape[2]), F32)
        for m in ht[c].order():
            ht[c].ready(m)
            weights(2, m)
            total += jnp.dot(hb[c, m], wd[m], preferred_element_type=F32)
        ob[c] = total.astype(BF16)
        for d in range(c * per, (c + 1) * per):
            if d:
                copy = r_copy(d)
                copy.start()
                sends.append(copy)

    def keys_ready():
        for d in range(1, n_ep):
            ep_copy(kb.at[0], kb.at[d], d, kz_send, kz_recv).wait_recv()
            ep_copy(vb.at[0], vb.at[d], d, vz_send, vz_recv).wait_recv()

    def attention(part):
        keys = n_ep * length
        block = length // 2
        rows = pl.ds(part * block, block)
        outs = []
        for h in range(q_ref.shape[1] // HEAD):
            g = h * KV_HEADS // Q_HEADS
            lane = pl.ds(g * HEAD, HEAD)
            query = qb[rows, pl.ds(h * HEAD, HEAD)]
            key = kb[:, :, lane].reshape(keys, HEAD)
            value = vb[:, :, lane].reshape(keys, HEAD)
            scores = lax.dot_general(
                query, key, (((1,), (1,)), ((), ())), preferred_element_type=F32
            )
            raw = jnp.exp(scores - jnp.max(scores, axis=1, keepdims=True))
            total = jnp.sum(raw, axis=1, keepdims=True)
            out = jnp.dot(raw.astype(BF16), value, preferred_element_type=F32)
            outs.append(out / total)
        mb[0, rows, :] = jnp.concatenate(outs, axis=1).astype(BF16)

    def project():
        total = jnp.zeros(att_ref.shape, F32)
        squares = jnp.zeros((length, 1), F32)
        for m in mt.order():
            mt.ready(m)
            weights(3, m)
            block = mb[m].astype(F32)
            squares += jnp.sum(block * block, axis=1, keepdims=True)
            scaled = (block * mg_ref[tp ^ m]).astype(BF16)
            total += jnp.dot(scaled, wo[m], preferred_element_type=F32)
        scale = lax.rsqrt(squares / mg_ref.shape[0] / mg_ref.shape[2] + EPS)
        att_ref[...] = (total * scale).astype(BF16)

    def combine():
        stack = jnp.concatenate(
            [slot_t[0].astype(F32), slot_t[1].astype(F32), rwt_ref[...]] * 2, axis=0
        )
        columns = lax.dot_general(
            jnp.where(i0 == i1, 1.0, 0.0).astype(F32), stack, (((1,), (1,)), ((), ())),
            precision=lax.Precision.HIGHEST, preferred_element_type=F32,
        )
        slot = [(columns[:, k : k + 1] + 0.5).astype(jnp.int32) for k in range(2)]
        total = [jnp.zeros(mix_ref.shape, F32) for k in range(2)]
        for d in range(n_ep):
            if d:
                r_copy(d).wait_recv()
                back = rb[d]
            else:
                back = ob[0, pl.ds(0, cap), :]
            index = (ep ^ d) * cap + iota((length, cap), 1)
            for k in range(2):
                choose = jnp.where(slot[k] == index, 1.0, 0.0).astype(BF16)
                total[k] += jnp.dot(choose, back, preferred_element_type=F32)
        mix_ref[...] = (total[0] * columns[:, 2:3] + total[1] * columns[:, 3:4]).astype(BF16)


    if per > 1:
        send_rows(1)
    send_rows(2)
    xt[0].stage(1)
    x_first(1)
    send_rows(3)
    xt[0].stage(2)
    turn_queries()
    hidden(0)
    ht[0].stage(0)
    xt[1].stage(1)
    ht[0].stage(1)
    xt[1].stage(2)
    x_first(2)
    send_keys()
    hidden(1)
    ht[1].stage(0)
    ht[0].stage(2)
    xt[2].stage(1)
    x_first(3)
    down(0)
    ht[1].stage(1)
    xt[2].stage(2)
    hidden(2)
    ht[2].stage(0)
    xt[3].stage(1)
    ht[1].stage(2)
    down(1)
    ht[2].stage(1)
    keys_ready()
    attention(0)
    xt[3].stage(2)
    ht[2].stage(2)
    hidden(3)
    ht[3].stage(0)
    down(2)
    attention(1)
    ht[3].stage(1)
    mt.stage(0)
    ht[3].stage(2)
    down(3)
    mt.stage(1)
    mt.stage(2)
    project()
    combine()

    for copy in sends:
        copy.wait_send()
    for gather in xt + ht + [mt]:
        gather.drain()


def hand_on(a_ref, b_ref, a_out, b_out):
    a_out[...] = a_ref[...]
    b_out[...] = b_ref[...]


def shards(
    n_ep, n_tp,
    queries, key_rows, values, query_gain, key_gain, mix_gain, out_weight, expert_input,
    expert_gain, route_ids, route_weights, expert_gate, expert_up, expert_down,
):
    length, width = expert_input.shape
    qw, kw = queries.shape[1], key_rows.shape[1]
    ffw = expert_gate.shape[2]
    out_w = out_weight.shape[1]
    copies = length * route_ids.shape[1]
    capacity = (4 * copies + 3 * n_ep - 1) // (3 * n_ep)
    cap = (capacity + 15) // 16 * 16
    groups = 4
    rows = cap * (n_ep // groups)
    plan = gather_plan(n_tp)

    table_w = min(128, qw)
    operands = (
        queries, key_rows, values,
        query_gain.reshape(1, HEAD), key_gain.reshape(1, HEAD),
        mix_gain.reshape(n_tp, 1, qw),
        out_weight.reshape(n_tp, qw, out_w),
        expert_input,
        expert_gain.reshape(n_tp, 1, width),
        route_ids.T, route_weights.T,
        expert_gate.reshape(n_tp, width, ffw),
        expert_up.reshape(n_tp, width, ffw),
        expert_down.reshape(n_tp, ffw, out_w),
    )
    vmem = pl.BlockSpec(memory_space=pltpu.VMEM)
    hbm = pl.BlockSpec(memory_space=pl.ANY)
    specs = [hbm if i in (6, 11, 12, 13) else vmem for i in range(len(operands))]
    dma = pltpu.SemaphoreType.DMA
    scratch = [
        pltpu.VMEM((length, table_w), F32),
        pltpu.VMEM((length, table_w), F32),
        pltpu.VMEM((n_ep, cap, width), BF16),
        pltpu.VMEM((groups, n_tp, rows, width), BF16),
        pltpu.VMEM((groups, n_tp, rows, ffw), BF16),
        pltpu.VMEM((n_tp, length, qw), BF16),
        pltpu.VMEM((n_ep, length, kw), BF16),
        pltpu.VMEM((n_ep, length, kw), BF16),
        pltpu.VMEM((length, qw), BF16),
        pltpu.VMEM((groups, rows, out_w), BF16),
        pltpu.VMEM((n_ep, cap, out_w), BF16),
        pltpu.VMEM((n_tp, width, 2 * ffw), BF16),
        pltpu.VMEM((n_tp, ffw, out_w), BF16),
        pltpu.VMEM((n_tp, qw, out_w), BF16),
        dma((4, n_tp)),
        dma((1,)),
    ]
    scratch += [dma((n_ep,))] * 8
    scratch += [dma((groups, len(plan)))] * 4 + [dma((len(plan),))] * 2
    outs = pl.pallas_call(
        functools.partial(kernel, n_ep, n_tp, cap, plan),
        out_shape=(
            jax.ShapeDtypeStruct((length, out_w), BF16),
            jax.ShapeDtypeStruct((length, out_w), BF16),
        ),
        in_specs=specs,
        out_specs=(vmem, vmem),
        scratch_shapes=scratch,
        compiler_params=pltpu.CompilerParams(
            collective_id=0, has_side_effects=True, vmem_limit_bytes=60 * 1024 * 1024
        ),
    )(*operands)
    return pl.pallas_call(
        hand_on,
        out_shape=tuple(jax.ShapeDtypeStruct(o.shape, o.dtype) for o in outs),
        in_specs=(vmem, vmem),
        out_specs=(vmem, vmem),
    )(*outs)


def solution(mesh):
    placed = (
        P("ep", "tp"), P("ep", "tp"), P("ep", "tp"), P(), P(), P(), P(None, "tp"),
        P("ep", "tp"), P(), P("ep", None), P("ep", None),
        P("ep", None, "tp"), P("ep", None, "tp"), P("ep", None, "tp"),
    )
    return jax.shard_map(
        functools.partial(shards, mesh.shape["ep"], mesh.shape["tp"]),
        mesh=mesh,
        in_specs=placed,
        out_specs=(P("ep", "tp"), P("ep", "tp")),
        check_vma=False,
    )
```

profile of v0, /device:TPU:0, one launch (start us, length us, event | category | flops | bytes accessed | tf_op | source)
XLA Modules:
  0.0 65.7 jit_solution(11892286732745259227)
XLA Ops:
  0.6 63.3 %shard_map.149 = (bf16[256,512]{1,0:T(8,128)(2,1)}, bf16[256,512]{1,0:T(8,128)(2,1)}) custom-call(bf16[256,256]{1,0:T(8,128)(2,1)} %q_ref.1, bf16[256,128]{1,0:T(8,128)(2,1)} %k_ref.1, bf16[256,128]{1,0:T(8,128)(2,1)} %v_ref.1, f32[1,64]{1,0:T(1,128)} %bitcast.18, f32[1,64]{1,0:T(1,128)} %bitcast.19, f32[8,1,256]{2,1,0:T(1,128)} %bitcast.15, ...), custom_call_target="tpu_custom_call" | custom-call | tf_op jit(solution)/shard_map/pallas_call | solution.py:480
  63.9 1.8 %shard_map.150 = (bf16[256,512]{1,0:T(8,128)(2,1)}, bf16[256,512]{1,0:T(8,128)(2,1)}) custom-call(bf16[256,512]{1,0:T(8,128)(2,1)} %get-tuple-element.4.a_ref, bf16[256,512]{1,0:T(8,128)(2,1)} %get-tuple-element.5.b_ref), custom_call_target="tpu_custom_call" | custom-call | tf_op jit(solution)/shard_map/pallas_call | solution.py:493
where the time goes:
time: 66.4 us; the launch traced here: 65.7 us
  Pallas kernels  65.1 us (98%)
    pallas_call x1, Pallas kernels, shards(): pl.pallas_call(functools.partial(kernel, n_ep, n_tp, cap, plan), out_shap...  63.3 us
    pallas_call x1, Pallas kernels, shards(): pl.pallas_call(hand_on, out_shape=tuple((jax.ShapeDtypeStruct(o.shape, o....  1.84 us

commit v1 on v0

--- a/solution.py
+++ b/solution.py
@@ -419,6 +419,380 @@
         gather.drain()
 
 
+RELAY_PLAN = (
+    (2, 0, 0),
+    (4, 0, 1),
+    (2, 0, 1),
+    (4, 0, 0),
+    (4, 2, 0),
+    (2, 4, 1),
+    (1, 0, None),
+    (1, 2, None),
+    (1, 4, None),
+    (1, 6, None),
+)
+RELAY_WAIT = (0, 0, 1, 1, 2, 2, 3, 3, 3, 3)
+OWN = (0, 1, 2, 3, 6)
+FORWARD = (4, 5)
+SIDE = (7, 8)
+CORNER = (9,)
+NEEDS = {FORWARD: 0, SIDE: 1, CORNER: 2}
+NEAR = (0, 2, 4, 6)
+FAR = (1, 3, 5, 7)
+
+
+class Relay:
+    def __init__(self, name, buf, send, recv, tp):
+        self.name = name
+        self.buf, self.send, self.recv, self.tp = buf, send, recv, tp
+        self.waited = set()
+
+    def part(self, block, half):
+        if half is None:
+            return self.buf.at[block]
+        width = self.buf.shape[-1] // 2
+        return self.buf.at[block, :, pl.ds(half * width, width)]
+
+    def copy(self, i):
+        target, block, half = RELAY_PLAN[i]
+        return pltpu.make_async_remote_copy(
+            src_ref=self.part(block, half),
+            dst_ref=self.part(block ^ target, half),
+            send_sem=self.send,
+            recv_sem=self.recv.at[RELAY_WAIT[i]],
+            device_id={"tp": self.tp ^ target},
+            device_id_type=MESH,
+        )
+
+    def whole(self, blocks, i):
+        part = self.buf.at[pl.ds(0, blocks)]
+        return pltpu.make_async_remote_copy(
+            src_ref=part, dst_ref=part, send_sem=self.send, recv_sem=self.recv.at[i],
+            device_id={"tp": self.tp ^ 1}, device_id_type=MESH,
+        )
+
+    def wait(self, i):
+        if i not in self.waited:
+            self.waited.add(i)
+            with jax.named_scope(f"w{self.name}_{i}"):
+                self.whole(len(FAR) if i == 3 else 1, i).wait_recv()
+
+    def issue(self, entries):
+        if entries in NEEDS:
+            self.wait(NEEDS[entries])
+        for i in entries:
+            self.copy(i).start()
+
+    def ready(self, block):
+        if block in FAR:
+            self.wait(3)
+        elif block:
+            for i in (0, 1, 2):
+                self.wait(i)
+
+    def drain(self):
+        self.whole(len(FAR) + 3, 0).wait_send()
+
+
+def line_kernel(
+    n_ep, n_tp, cap,
+    q_ref, k_ref, v_ref, qg_ref, kg_ref, mg_ref, wo_hbm, x_ref, xg_ref,
+    idst_ref, rwt_ref, wg_hbm, wu_hbm, wd_hbm,
+    att_ref, mix_ref,
+    cos_ref, sin_ref, xo, xb, hb, mb, kv, qb, ob, rb, ct, wgu, wd, wo,
+    w_sem, z_send, z_recv, t_send, t_recv,
+):
+    ep, tp = lax.axis_index("ep"), lax.axis_index("tp")
+    length = x_ref.shape[0]
+    ffw = hb.shape[-1]
+    kw = k_ref.shape[1]
+    inner = (ep + 1) // 2 % 2
+    order = (0, 1 + inner, 2 - inner, 3)
+
+    barrier = pltpu.get_barrier_semaphore()
+    for d in range(1, n_ep):
+        pl.semaphore_signal(barrier, inc=1, device_id={"ep": ep ^ d}, device_id_type=MESH)
+    for m in range(1, n_tp):
+        pl.semaphore_signal(barrier, inc=1, device_id={"tp": tp ^ m}, device_id_type=MESH)
+
+    lanes = (n_ep + 15) // 16 * 16
+    hit_t = [(idst_ref[k : k + 1, :] == iota((lanes, length), 0)) for k in range(2)]
+    both_t = sum(jnp.where(h, 1.0, 0.0) for h in hit_t).astype(BF16)
+    i0, i1 = iota((length, length), 0), iota((length, length), 1)
+    before_t = jnp.where(i0 < i1, 1.0, 0.0).astype(BF16)
+    count_t = jnp.dot(both_t, before_t, preferred_element_type=F32)
+    slot_t = [
+        jnp.sum(jnp.where(hit_t[k], count_t, 0.0), axis=0, keepdims=True).astype(jnp.int32)
+        + idst_ref[k : k + 1, :] * cap
+        for k in range(2)
+    ]
+
+    def picked_rows(d):
+        index = (ep ^ d) * cap + iota((cap, length), 0)
+        choose = jnp.where((slot_t[0] == index) | (slot_t[1] == index), 1.0, 0.0).astype(BF16)
+        return jnp.dot(choose, x_ref[...], preferred_element_type=F32).astype(BF16)
+
+    def ep_copy(source, target, d, send, recv):
+        return pltpu.make_async_remote_copy(
+            src_ref=source, dst_ref=target, send_sem=send, recv_sem=recv,
+            device_id={"ep": ep ^ d}, device_id_type=MESH,
+        )
+
+    def x_copy(d):
+        return ep_copy(xo.at[d], xb.at[d, 0], d, z_send.at[0], z_recv.at[0, d])
+
+    def r_copy(d):
+        return ep_copy(ob.at[d], rb.at[d], d, z_send.at[1], z_recv.at[1, d])
+
+    def kv_copy(i):
+        d, block = ((1, 0), (2, 0), (1, 2))[i]
+        return ep_copy(kv.at[block], kv.at[block ^ d], d, z_send.at[2], z_recv.at[2, i])
+
+    xt = [
+        Relay(f"x{j}", xb.at[order[j]], t_send.at[0, order[j]], t_recv.at[0, order[j]], tp)
+        for j in range(n_ep)
+    ]
+    ht = [
+        Relay(f"h{d}", hb.at[d], t_send.at[1, d], t_recv.at[1, d], tp)
+        for d in range(n_ep)
+    ]
+    mt = Relay("m", mb, t_send.at[2, 0], t_recv.at[2, 0], tp)
+
+    pieces = (
+        (wg_hbm, wgu.at[:, :, pl.ds(0, ffw)]),
+        (wu_hbm, wgu.at[:, :, pl.ds(ffw, ffw)]),
+        (wd_hbm, wd),
+        (wo_hbm, wo),
+    )
+    local = [
+        pltpu.make_async_copy(source, target, w_sem.at[k])
+        for k, (source, target) in enumerate(pieces)
+    ]
+    fetched = set()
+
+    def weights(k):
+        if k not in fetched:
+            fetched.add(k)
+            with jax.named_scope(f"ww_{k}"):
+                local[k].wait()
+
+    def own_keys():
+        tables(cos_ref, sin_ref, ep * length)
+        kv[0, :, pl.ds(kw, kw)] = v_ref[...]
+        kv[0, :, pl.ds(0, kw)] = norm_turn(
+            k_ref[...],
+            jnp.concatenate([kg_ref[...]] * (kw // HEAD), axis=1),
+            cos_ref[:, :kw],
+            sin_ref[:, :kw],
+        ).astype(BF16)
+
+    def send_keys():
+        kv_copy(0).start()
+        kv_copy(1).start()
+
+    def keys_on():
+        with jax.named_scope("wkv_1"):
+            kv_copy(1).wait_recv()
+        kv_copy(2).start()
+
+    def keys_ready():
+        with jax.named_scope("wkv_0"):
+            kv_copy(0).wait_recv()
+        with jax.named_scope("wkv_2"):
+            kv_copy(2).wait_recv()
+
+    def turn_queries():
+        qw = cos_ref.shape[1]
+        gain = jnp.concatenate([qg_ref[...]] * (qw // HEAD), axis=1)
+        for i in range(q_ref.shape[1] // qw):
+            part = pl.ds(i * qw, qw)
+            turned = norm_turn(q_ref[:, part], gain, cos_ref[...], sin_ref[...])
+            qb[:, part] = (turned.astype(BF16).astype(F32) * (1.0 / math.sqrt(HEAD))).astype(BF16)
+
+    def x_arrived(j):
+        with jax.named_scope(f"wxz_{j}"):
+            x_copy(order[j]).wait_recv()
+
+    def hidden(j):
+        d = order[j]
+        total = jnp.zeros((cap, 2 * ffw), F32)
+        squares = jnp.zeros((cap, 1), F32)
+        for m in NEAR + FAR:
+            xt[j].ready(m)
+            weights(0)
+            weights(1)
+            block = xb[d, m].astype(F32)
+            squares += jnp.sum(block * block, axis=1, keepdims=True)
+            scaled = (block * xg_ref[tp ^ m]).astype(BF16)
+            total += jnp.dot(scaled, wgu[tp ^ m], preferred_element_type=F32)
+        stat = lax.rsqrt(squares / xg_ref.shape[0] / xg_ref.shape[2] + EPS)
+        gate = total[:, :ffw] * stat
+        up = total[:, ffw:] * stat
+        hb[d, 0] = (gate / (1.0 + jnp.exp(-gate)) * up).astype(BF16)
+
+    def down(d):
+        total = jnp.zeros((ob.shape[1], ob.shape[2]), F32)
+        for m in NEAR + FAR:
+            ht[d].ready(m)
+            weights(2)
+            total += jnp.dot(hb[d, m], wd[tp ^ m], preferred_element_type=F32)
+        ob[d] = total.astype(BF16)
+        if d:
+            r_copy(d).start()
+
+    def attention(part, pair):
+        keys = n_ep * length
+        block = length // 2
+        rows = pl.ds(part * block, block)
+        outs = []
+        for h in range(2 * pair, 2 * pair + 2):
+            g = h * KV_HEADS // Q_HEADS
+            query = qb[rows, pl.ds(h * HEAD, HEAD)]
+            key = kv[:, :, pl.ds(g * HEAD, HEAD)].reshape(keys, HEAD)
+            value = kv[:, :, pl.ds(kw + g * HEAD, HEAD)].reshape(keys, HEAD)
+            scores = lax.dot_general(
+                query, key, (((1,), (1,)), ((), ())), preferred_element_type=F32
+            )
+            raw = jnp.exp(scores - jnp.max(scores, axis=1, keepdims=True))
+            total = jnp.sum(raw, axis=1, keepdims=True)
+            out = jnp.dot(raw.astype(BF16), value, preferred_element_type=F32)
+            outs.append(out / total)
+        lane = pl.ds(2 * pair * HEAD, 2 * HEAD)
+        mb[0, rows, lane] = jnp.concatenate(outs, axis=1).astype(BF16)
+
+    def project():
+        total = jnp.zeros(att_ref.shape, F32)
+        squares = jnp.zeros((length, 1), F32)
+        for m in NEAR + FAR:
+            mt.ready(m)
+            weights(3)
+            block = mb[m].astype(F32)
+            squares += jnp.sum(block * block, axis=1, keepdims=True)
+            scaled = (block * mg_ref[tp ^ m]).astype(BF16)
+            total += jnp.dot(scaled, wo[tp ^ m], preferred_element_type=F32)
+        scale = lax.rsqrt(squares / mg_ref.shape[0] / mg_ref.shape[2] + EPS)
+        att_ref[...] = (total * scale).astype(BF16)
+
+    places = {}
+
+    def columns():
+        stack = jnp.concatenate(
+            [slot_t[0].astype(F32), slot_t[1].astype(F32), rwt_ref[...]] * 2, axis=0
+        )
+        column = lax.dot_general(
+            jnp.where(i0 == i1, 1.0, 0.0).astype(F32), stack, (((1,), (1,)), ((), ())),
+            precision=lax.Precision.HIGHEST, preferred_element_type=F32,
+        )
+        places["slot"] = [(column[:, k : k + 1] + 0.5).astype(jnp.int32) for k in range(2)]
+        places["weight"] = [column[:, 2 + k : 3 + k] for k in range(2)]
+
+    def combine(d, first=False, last=False):
+        if d:
+            with jax.named_scope(f"wr_{d}"):
+                r_copy(d).wait_recv()
+        back = rb[d] if d else ob[0]
+        index = (ep ^ d) * cap + iota((length, cap), 1)
+        total = []
+        for k in range(2):
+            choose = jnp.where(places["slot"][k] == index, 1.0, 0.0).astype(BF16)
+            found = jnp.dot(choose, back, preferred_element_type=F32)
+            total.append(found if first else ct[k] + found)
+        if last:
+            weight = places["weight"]
+            mix_ref[...] = (total[0] * weight[0] + total[1] * weight[1]).astype(BF16)
+        else:
+            for k in range(2):
+                ct[k] = total[k]
+
+    def step(name, f, *args, **kwargs):
+        with jax.named_scope("S_" + name):
+            f(*args, **kwargs)
+
+    def send_x(d):
+        xo[d] = picked_rows(d)
+        x_copy(d).start()
+
+    for copy in local:
+        copy.start()
+    xb[0, 0] = picked_rows(0)
+    with jax.named_scope("S_barrier"):
+        pl.semaphore_wait(barrier, n_ep + n_tp - 2)
+    step("X0own", xt[0].issue, OWN)
+    step("sx2", send_x, 2)
+    step("sx1", send_x, 1)
+    step("keys", own_keys)
+    step("X0fwd", xt[0].issue, FORWARD)
+    step("X0side", xt[0].issue, SIDE)
+    step("columns", columns)
+    step("ax1", x_arrived, 1)
+    step("X1own", xt[1].issue, OWN)
+    step("sx3", send_x, 3)
+    step("X0cor", xt[0].issue, CORNER)
+    step("hid0", hidden, 0)
+    step("X1fwd", xt[1].issue, FORWARD)
+    step("ax2", x_arrived, 2)
+    step("X2own", xt[2].issue, OWN)
+    step("X1side", xt[1].issue, SIDE)
+    step("X1cor", xt[1].issue, CORNER)
+    step("X2fwd", xt[2].issue, FORWARD)
+    step("ax3", x_arrived, 3)
+    step("X3own", xt[3].issue, OWN)
+    step("hid1", hidden, 1)
+    step("sendkv", send_keys)
+    step("X2side", xt[2].issue, SIDE)
+    step("queries", turn_queries)
+    step("X2cor", xt[2].issue, CORNER)
+    step("X3fwd", xt[3].issue, FORWARD)
+    step("hid2", hidden, 2)
+    step("H2own", ht[2].issue, OWN)
+    step("H1own", ht[1].issue, OWN)
+    step("X3side", xt[3].issue, SIDE)
+    step("X3cor", xt[3].issue, CORNER)
+    step("keyson", keys_on)
+    step("H2fwd", ht[2].issue, FORWARD)
+    step("hid3", hidden, 3)
+    step("H3own", ht[3].issue, OWN)
+    step("H1fwd", ht[1].issue, FORWARD)
+    step("H2side", ht[2].issue, SIDE)
+    step("H2cor", ht[2].issue, CORNER)
+    step("wkv", keys_ready)
+    step("att00", attention, 0, 0)
+    step("att01", attention, 0, 1)
+    step("H3fwd", ht[3].issue, FORWARD)
+    step("down2", down, 2)
+    step("att10", attention, 1, 0)
+    step("H1side", ht[1].issue, SIDE)
+    step("H1cor", ht[1].issue, CORNER)
+    step("att11", attention, 1, 1)
+    step("Mown", mt.issue, OWN)
+    step("H3side", ht[3].issue, SIDE)
+    step("down1", down, 1)
+    step("H3cor", ht[3].issue, CORNER)
+    step("H0own", ht[0].issue, OWN)
+    step("down3", down, 3)
+    step("Mfwd", mt.issue, FORWARD)
+    step("Mside", mt.issue, SIDE)
+    step("H0fwd", ht[0].issue, FORWARD)
+    step("Mcor", mt.issue, CORNER)
+    step("H0side", ht[0].issue, SIDE)
+    step("H0cor", ht[0].issue, CORNER)
+    step("project", project)
+    step("down0", down, 0)
+    step("comb0F", combine, 0, first=True)
+    step("comb1", combine, 1)
+    step("comb2", combine, 2)
+    step("comb3L", combine, 3, last=True)
+
+    with jax.named_scope("S_drain"):
+        for i, buf in enumerate((xo, rb, kv)):
+            ep_copy(
+                buf.at[pl.ds(0, n_ep - 1)], buf.at[pl.ds(0, n_ep - 1)], 1,
+                z_send.at[i], z_recv.at[i, 0],
+            ).wait_send()
+        for gather in xt + ht + [mt]:
+            gather.drain()
+
+
 def hand_on(a_ref, b_ref, a_out, b_out):
     a_out[...] = a_ref[...]
     b_out[...] = b_ref[...]
@@ -457,28 +831,37 @@
     hbm = pl.BlockSpec(memory_space=pl.ANY)
     specs = [hbm if i in (6, 11, 12, 13) else vmem for i in range(len(operands))]
     dma = pltpu.SemaphoreType.DMA
-    scratch = [
-        pltpu.VMEM((length, table_w), F32),
-        pltpu.VMEM((length, table_w), F32),
+    line = n_ep == 4 and n_tp == 8
+    tables_at = [pltpu.VMEM((length, table_w), F32)] * 2
+    blocks_at = [
         pltpu.VMEM((n_ep, cap, width), BF16),
         pltpu.VMEM((groups, n_tp, rows, width), BF16),
         pltpu.VMEM((groups, n_tp, rows, ffw), BF16),
         pltpu.VMEM((n_tp, length, qw), BF16),
-        pltpu.VMEM((n_ep, length, kw), BF16),
-        pltpu.VMEM((n_ep, length, kw), BF16),
+    ]
+    weights_at = [
+        pltpu.VMEM((n_tp, width, 2 * ffw), BF16),
+        pltpu.VMEM((n_tp, ffw, out_w), BF16),
+        pltpu.VMEM((n_tp, qw, out_w), BF16),
+    ]
+    results_at = [
         pltpu.VMEM((length, qw), BF16),
         pltpu.VMEM((groups, rows, out_w), BF16),
         pltpu.VMEM((n_ep, cap, out_w), BF16),
-        pltpu.VMEM((n_tp, width, 2 * ffw), BF16),
-        pltpu.VMEM((n_tp, ffw, out_w), BF16),
-        pltpu.VMEM((n_tp, qw, out_w), BF16),
-        dma((4, n_tp)),
-        dma((1,)),
     ]
-    scratch += [dma((n_ep,))] * 8
-    scratch += [dma((groups, len(plan)))] * 4 + [dma((len(plan),))] * 2
+    if line:
+        body = functools.partial(line_kernel, n_ep, n_tp, cap)
+        scratch = tables_at + blocks_at + [pltpu.VMEM((n_ep, length, 2 * kw), BF16)]
+        scratch += results_at + [pltpu.VMEM((2, length, out_w), F32)] + weights_at
+        scratch += [dma((4,)), dma((3,)), dma((3, n_ep)), dma((3, n_ep)), dma((3, n_ep, 4))]
+    else:
+        body = functools.partial(kernel, n_ep, n_tp, cap, plan)
+        scratch = tables_at + blocks_at + [pltpu.VMEM((n_ep, length, kw), BF16)] * 2
+        scratch += results_at + weights_at
+        scratch += [dma((4, n_tp)), dma((1,))] + [dma((n_ep,))] * 8
+        scratch += [dma((groups, len(plan)))] * 4 + [dma((len(plan),))] * 2
     outs = pl.pallas_call(
-        functools.partial(kernel, n_ep, n_tp, cap, plan),
+        body,
         out_shape=(
             jax.ShapeDtypeStruct((length, out_w), BF16),
             jax.ShapeDtypeStruct((length, out_w), BF16),

time: 66.4 us -> 60.7 us (0.914)
  Pallas kernels: 65.1 us -> 59.9 us
    pallas_call x1, Pallas kernels: 63.3 us -> 58 us  [shards(): pl.pallas_call(body, out_shape=(jax.ShapeDtypeStruct((length, out_w), BF1...]
where the time goes in v1:
time: 60.7 us; the launch traced here: 60.5 us
  Pallas kernels  59.9 us (99%)
  between operations  0.64 us (1%)
    pallas_call x1, Pallas kernels, shards(): pl.pallas_call(body, out_shape=(jax.ShapeDtypeStruct((length, out_w), BF1...  58 us
    pallas_call x1, Pallas kernels, shards(): pl.pallas_call(hand_on, out_shape=tuple((jax.ShapeDtypeStruct(o.shape, o....  1.84 us

profile of v1, /device:TPU:0, one launch (start us, length us, event | category | flops | bytes accessed | tf_op | source)
XLA Modules:
  0.0 60.5 jit_solution(16193617953389716209)
XLA Ops:
  0.6 58.0 %shard_map.149 = (bf16[256,512]{1,0:T(8,128)(2,1)}, bf16[256,512]{1,0:T(8,128)(2,1)}) custom-call(bf16[256,256]{1,0:T(8,128)(2,1)} %q_ref.1, bf16[256,128]{1,0:T(8,128)(2,1)} %k_ref.1, bf16[256,128]{1,0:T(8,128)(2,1)} %v_ref.1, f32[1,64]{1,0:T(1,128)} %bitcast.18, f32[1,64]{1,0:T(1,128)} %bitcast.19, f32[8,1,256]{2,1,0:T(1,128)} %bitcast.15, ...), custom_call_target="tpu_custom_call" | custom-call | tf_op jit(solution)/shard_map/pallas_call | solution.py:863
  58.7 1.8 %shard_map.150 = (bf16[256,512]{1,0:T(8,128)(2,1)}, bf16[256,512]{1,0:T(8,128)(2,1)}) custom-call(bf16[256,512]{1,0:T(8,128)(2,1)} %get-tuple-element.4.a_ref, bf16[256,512]{1,0:T(8,128)(2,1)} %get-tuple-element.5.b_ref), custom_call_target="tpu_custom_call" | custom-call | tf_op jit(solution)/shard_map/pallas_call | solution.py:876

commit v2 on v1

--- a/solution.py
+++ b/solution.py
@@ -1,5 +1,6 @@
 import functools
 import math
+import types
 
 import jax
 import jax.numpy as jnp
@@ -433,6 +434,8 @@
 )
 RELAY_WAIT = (0, 0, 1, 1, 2, 2, 3, 3, 3, 3)
 OWN = (0, 1, 2, 3, 6)
+LEAD = (0, 1)
+REST = (2, 3, 6)
 FORWARD = (4, 5)
 SIDE = (7, 8)
 CORNER = (9,)
@@ -506,8 +509,8 @@
     length = x_ref.shape[0]
     ffw = hb.shape[-1]
     kw = k_ref.shape[1]
+    half = length // 2
     inner = (ep + 1) // 2 % 2
-    order = (0, 1 + inner, 2 - inner, 3)
 
     barrier = pltpu.get_barrier_semaphore()
     for d in range(1, n_ep):
@@ -548,15 +551,22 @@
         d, block = ((1, 0), (2, 0), (1, 2))[i]
         return ep_copy(kv.at[block], kv.at[block ^ d], d, z_send.at[2], z_recv.at[2, i])
 
-    xt = [
-        Relay(f"x{j}", xb.at[order[j]], t_send.at[0, order[j]], t_recv.at[0, order[j]], tp)
-        for j in range(n_ep)
-    ]
-    ht = [
-        Relay(f"h{d}", hb.at[d], t_send.at[1, d], t_recv.at[1, d], tp)
-        for d in range(n_ep)
-    ]
-    mt = Relay("m", mb, t_send.at[2, 0], t_recv.at[2, 0], tp)
+    live = types.SimpleNamespace()
+
+    def fresh():
+        live.fetched = set()
+        live.xt = [
+            Relay(f"x{d}", xb.at[d], t_send.at[0, d], t_recv.at[0, d], tp) for d in range(n_ep)
+        ]
+        live.ht = [
+            Relay(f"h{d}", hb.at[d], t_send.at[1, d], t_recv.at[1, d], tp) for d in range(n_ep)
+        ]
+        live.mt = [
+            Relay(
+                f"m{k}", mb.at[:, pl.ds(k * half, half)], t_send.at[2, k], t_recv.at[2, k], tp
+            )
+            for k in range(2)
+        ]
 
     pieces = (
         (wg_hbm, wgu.at[:, :, pl.ds(0, ffw)]),
@@ -568,11 +578,9 @@
         pltpu.make_async_copy(source, target, w_sem.at[k])
         for k, (source, target) in enumerate(pieces)
     ]
-    fetched = set()
-
     def weights(k):
-        if k not in fetched:
-            fetched.add(k)
+        if k not in live.fetched:
+            live.fetched.add(k)
             with jax.named_scope(f"ww_{k}"):
                 local[k].wait()
 
@@ -609,16 +617,15 @@
             turned = norm_turn(q_ref[:, part], gain, cos_ref[...], sin_ref[...])
             qb[:, part] = (turned.astype(BF16).astype(F32) * (1.0 / math.sqrt(HEAD))).astype(BF16)
 
-    def x_arrived(j):
-        with jax.named_scope(f"wxz_{j}"):
-            x_copy(order[j]).wait_recv()
-
-    def hidden(j):
-        d = order[j]
+    def x_arrived(d):
+        with jax.named_scope(f"wxz_{d}"):
+            x_copy(d).wait_recv()
+
+    def hidden(d):
         total = jnp.zeros((cap, 2 * ffw), F32)
         squares = jnp.zeros((cap, 1), F32)
         for m in NEAR + FAR:
-            xt[j].ready(m)
+            live.xt[d].ready(m)
             weights(0)
             weights(1)
             block = xb[d, m].astype(F32)
@@ -633,7 +640,7 @@
     def down(d):
         total = jnp.zeros((ob.shape[1], ob.shape[2]), F32)
         for m in NEAR + FAR:
-            ht[d].ready(m)
+            live.ht[d].ready(m)
             weights(2)
             total += jnp.dot(hb[d, m], wd[tp ^ m], preferred_element_type=F32)
         ob[d] = total.astype(BF16)
@@ -642,8 +649,7 @@
 
     def attention(part, pair):
         keys = n_ep * length
-        block = length // 2
-        rows = pl.ds(part * block, block)
+        rows = pl.ds(part * half, half)
         outs = []
         for h in range(2 * pair, 2 * pair + 2):
             g = h * KV_HEADS // Q_HEADS
@@ -660,18 +666,19 @@
         lane = pl.ds(2 * pair * HEAD, 2 * HEAD)
         mb[0, rows, lane] = jnp.concatenate(outs, axis=1).astype(BF16)
 
-    def project():
-        total = jnp.zeros(att_ref.shape, F32)
-        squares = jnp.zeros((length, 1), F32)
+    def project(part):
+        rows = pl.ds(part * half, half)
+        total = jnp.zeros((half, att_ref.shape[1]), F32)
+        squares = jnp.zeros((half, 1), F32)
         for m in NEAR + FAR:
-            mt.ready(m)
+            live.mt[part].ready(m)
             weights(3)
-            block = mb[m].astype(F32)
+            block = mb[m, rows, :].astype(F32)
             squares += jnp.sum(block * block, axis=1, keepdims=True)
             scaled = (block * mg_ref[tp ^ m]).astype(BF16)
             total += jnp.dot(scaled, wo[tp ^ m], preferred_element_type=F32)
         scale = lax.rsqrt(squares / mg_ref.shape[0] / mg_ref.shape[2] + EPS)
-        att_ref[...] = (total * scale).astype(BF16)
+        att_ref[rows, :] = (total * scale).astype(BF16)
 
     places = {}
 
@@ -712,90 +719,187 @@
         xo[d] = picked_rows(d)
         x_copy(d).start()
 
+    def finish():
+        with jax.named_scope("S_drain"):
+            for i, buf in enumerate((xo, rb, kv)):
+                part = buf.at[pl.ds(0, n_ep - 1)]
+                ep_copy(part, part, 1, z_send.at[i], z_recv.at[i, 0]).wait_send()
+            for gather in live.xt + live.ht + live.mt:
+                gather.drain()
+
     for copy in local:
         copy.start()
     xb[0, 0] = picked_rows(0)
     with jax.named_scope("S_barrier"):
         pl.semaphore_wait(barrier, n_ep + n_tp - 2)
-    step("X0own", xt[0].issue, OWN)
+    fresh()
+    step("X0own", live.xt[0].issue, OWN)
     step("sx2", send_x, 2)
     step("sx1", send_x, 1)
     step("keys", own_keys)
-    step("X0fwd", xt[0].issue, FORWARD)
-    step("X0side", xt[0].issue, SIDE)
     step("columns", columns)
-    step("ax1", x_arrived, 1)
-    step("X1own", xt[1].issue, OWN)
-    step("sx3", send_x, 3)
-    step("X0cor", xt[0].issue, CORNER)
-    step("hid0", hidden, 0)
-    step("X1fwd", xt[1].issue, FORWARD)
-    step("ax2", x_arrived, 2)
-    step("X2own", xt[2].issue, OWN)
-    step("X1side", xt[1].issue, SIDE)
-    step("X1cor", xt[1].issue, CORNER)
-    step("X2fwd", xt[2].issue, FORWARD)
-    step("ax3", x_arrived, 3)
-    step("X3own", xt[3].issue, OWN)
-    step("hid1", hidden, 1)
-    step("sendkv", send_keys)
-    step("X2side", xt[2].issue, SIDE)
-    step("queries", turn_queries)
-    step("X2cor", xt[2].issue, CORNER)
-    step("X3fwd", xt[3].issue, FORWARD)
-    step("hid2", hidden, 2)
-    step("H2own", ht[2].issue, OWN)
-    step("H1own", ht[1].issue, OWN)
-    step("X3side", xt[3].issue, SIDE)
-    step("X3cor", xt[3].issue, CORNER)
-    step("keyson", keys_on)
-    step("H2fwd", ht[2].issue, FORWARD)
-    step("hid3", hidden, 3)
-    step("H3own", ht[3].issue, OWN)
-    step("H1fwd", ht[1].issue, FORWARD)
-    step("H2side", ht[2].issue, SIDE)
-    step("H2cor", ht[2].issue, CORNER)
-    step("wkv", keys_ready)
-    step("att00", attention, 0, 0)
-    step("att01", attention, 0, 1)
-    step("H3fwd", ht[3].issue, FORWARD)
-    step("down2", down, 2)
-    step("att10", attention, 1, 0)
-    step("H1side", ht[1].issue, SIDE)
-    step("H1cor", ht[1].issue, CORNER)
-    step("att11", attention, 1, 1)
-    step("Mown", mt.issue, OWN)
-    step("H3side", ht[3].issue, SIDE)
-    step("down1", down, 1)
-    step("H3cor", ht[3].issue, CORNER)
-    step("H0own", ht[0].issue, OWN)
-    step("down3", down, 3)
-    step("Mfwd", mt.issue, FORWARD)
-    step("Mside", mt.issue, SIDE)
-    step("H0fwd", ht[0].issue, FORWARD)
-    step("Mcor", mt.issue, CORNER)
-    step("H0side", ht[0].issue, SIDE)
-    step("H0cor", ht[0].issue, CORNER)
-    step("project", project)
-    step("down0", down, 0)
-    step("comb0F", combine, 0, first=True)
-    step("comb1", combine, 1)
-    step("comb2", combine, 2)
-    step("comb3L", combine, 3, last=True)
-
-    with jax.named_scope("S_drain"):
-        for i, buf in enumerate((xo, rb, kv)):
-            ep_copy(
-                buf.at[pl.ds(0, n_ep - 1)], buf.at[pl.ds(0, n_ep - 1)], 1,
-                z_send.at[i], z_recv.at[i, 0],
-            ).wait_send()
-        for gather in xt + ht + [mt]:
-            gather.drain()
-
-
-def hand_on(a_ref, b_ref, a_out, b_out):
-    a_out[...] = a_ref[...]
-    b_out[...] = b_ref[...]
+
+    @pl.when(inner == 1)
+    def _():
+        fresh()
+        step("X0fwd", live.xt[0].issue, FORWARD)
+        step("X0side", live.xt[0].issue, SIDE)
+        step("ax2", x_arrived, 2)
+        step("X2own", live.xt[2].issue, OWN)
+        step("sx3", send_x, 3)
+        step("X0cor", live.xt[0].issue, CORNER)
+        step("hid0", hidden, 0)
+        step("X2fwd", live.xt[2].issue, FORWARD)
+        step("ax1", x_arrived, 1)
+        step("X1own", live.xt[1].issue, OWN)
+        step("X2side", live.xt[2].issue, SIDE)
+        step("X2cor", live.xt[2].issue, CORNER)
+        step("X1fwd", live.xt[1].issue, FORWARD)
+        step("hid2", hidden, 2)
+        step("H2own", live.ht[2].issue, OWN)
+        step("ax3", x_arrived, 3)
+        step("sendkv", send_keys)
+        step("X3lead", live.xt[3].issue, LEAD)
+        step("X1side", live.xt[1].issue, SIDE)
+        step("X1cor", live.xt[1].issue, CORNER)
+        step("H2fwd", live.ht[2].issue, FORWARD)
+        step("X3rest", live.xt[3].issue, REST)
+        step("H2side", live.ht[2].issue, SIDE)
+        step("queries", turn_queries)
+        step("keyson", keys_on)
+        step("hid1", hidden, 1)
+        step("X3fwd", live.xt[3].issue, FORWARD)
+        step("H1own", live.ht[1].issue, OWN)
+        step("H2cor", live.ht[2].issue, CORNER)
+        step("down2", down, 2)
+        step("X3side", live.xt[3].issue, SIDE)
+        step("wkv", keys_ready)
+        step("att00", attention, 0, 0)
+        step("X3cor", live.xt[3].issue, CORNER)
+        step("H1fwd", live.ht[1].issue, FORWARD)
+        step("hid3", hidden, 3)
+        step("H3own", live.ht[3].issue, OWN)
+        step("H1side", live.ht[1].issue, SIDE)
+        step("att01", attention, 0, 1)
+        step("M0own", live.mt[0].issue, OWN)
+        step("H1cor", live.ht[1].issue, CORNER)
+        step("att10", attention, 1, 0)
+        step("H3fwd", live.ht[3].issue, FORWARD)
+        step("H0own", live.ht[0].issue, OWN)
+        step("down1", down, 1)
+        step("att11", attention, 1, 1)
+        step("M0fwd", live.mt[0].issue, FORWARD)
+        step("M1own", live.mt[1].issue, OWN)
+        step("H3side", live.ht[3].issue, SIDE)
+        step("H3cor", live.ht[3].issue, CORNER)
+        step("M0side", live.mt[0].issue, SIDE)
+        step("down3", down, 3)
+        step("H0fwd", live.ht[0].issue, FORWARD)
+        step("M0cor", live.mt[0].issue, CORNER)
+        step("M1fwd", live.mt[1].issue, FORWARD)
+        step("H0side", live.ht[0].issue, SIDE)
+        step("H0cor", live.ht[0].issue, CORNER)
+        step("project0", project, 0)
+        step("M1side", live.mt[1].issue, SIDE)
+        step("down0", down, 0)
+        step("comb0F", combine, 0, first=True)
+        step("M1cor", live.mt[1].issue, CORNER)
+        step("comb2", combine, 2)
+        step("comb1", combine, 1)
+        step("project1", project, 1)
+        step("comb3L", combine, 3, last=True)
+        finish()
+
+    @pl.when(inner == 0)
+    def _():
+        fresh()
+        step("X0fwd", live.xt[0].issue, FORWARD)
+        step("X0side", live.xt[0].issue, SIDE)
+        step("ax1", x_arrived, 1)
+        step("X1own", live.xt[1].issue, OWN)
+        step("sx3", send_x, 3)
+        step("X0cor", live.xt[0].issue, CORNER)
+        step("hid0", hidden, 0)
+        step("X1fwd", live.xt[1].issue, FORWARD)
+        step("ax2", x_arrived, 2)
+        step("X2own", live.xt[2].issue, OWN)
+        step("X1side", live.xt[1].issue, SIDE)
+        step("X1cor", live.xt[1].issue, CORNER)
+        step("X2fwd", live.xt[2].issue, FORWARD)
+        step("ax3", x_arrived, 3)
+        step("X3own", live.xt[3].issue, OWN)
+        step("sendkv", send_keys)
+        step("hid1", hidden, 1)
+        step("X2side", live.xt[2].issue, SIDE)
+        step("queries", turn_queries)
+        step("X2cor", live.xt[2].issue, CORNER)
+        step("X3fwd", live.xt[3].issue, FORWARD)
+        step("hid2", hidden, 2)
+        step("H2own", live.ht[2].issue, OWN)
+        step("H1own", live.ht[1].issue, OWN)
+        step("X3side", live.xt[3].issue, SIDE)
+        step("keyson", keys_on)
+        step("X3cor", live.xt[3].issue, CORNER)
+        step("H2fwd", live.ht[2].issue, FORWARD)
+        step("hid3", hidden, 3)
+        step("H3own", live.ht[3].issue, OWN)
+        step("H2side", live.ht[2].issue, SIDE)
+        step("H1fwd", live.ht[1].issue, FORWARD)
+        step("wkv", keys_ready)
+        step("att00", attention, 0, 0)
+        step("H2cor", live.ht[2].issue, CORNER)
+        step("down2", down, 2)
+        step("H1side", live.ht[1].issue, SIDE)
+        step("H3fwd", live.ht[3].issue, FORWARD)
+        step("att01", attention, 0, 1)
+        step("M0own", live.mt[0].issue, OWN)
+        step("H0own", live.ht[0].issue, OWN)
+        step("H1cor", live.ht[1].issue, CORNER)
+        step("att10", attention, 1, 0)
+        step("H3side", live.ht[3].issue, SIDE)
+        step("att11", attention, 1, 1)
+        step("M1own", live.mt[1].issue, OWN)
+        step("H3cor", live.ht[3].issue, CORNER)
+        step("down3", down, 3)
+        step("M0fwd", live.mt[0].issue, FORWARD)
+        step("down1", down, 1)
+        step("M0side", live.mt[0].issue, SIDE)
+        step("H0fwd", live.ht[0].issue, FORWARD)
+        step("M1fwd", live.mt[1].issue, FORWARD)
+        step("M0cor", live.mt[0].issue, CORNER)
+        step("H0side", live.ht[0].issue, SIDE)
+        step("H0cor", live.ht[0].issue, CORNER)
+        step("project0", project, 0)
+        step("M1side", live.mt[1].issue, SIDE)
+        step("down0", down, 0)
+        step("comb0F", combine, 0, first=True)
+        step("comb1", combine, 1)
+        step("M1cor", live.mt[1].issue, CORNER)
+        step("comb2", combine, 2)
+        step("project1", project, 1)
+        step("comb3L", combine, 3, last=True)
+        finish()
+
+
+def hand_on(a_ref, b_ref, a_out, b_out, sems):
+    copies = [
+        pltpu.make_async_copy(a_ref, a_out, sems.at[0]),
+        pltpu.make_async_copy(b_ref, b_out, sems.at[1]),
+    ]
+    for copy in copies:
+        copy.start()
+    for copy in copies:
+        copy.wait()
+
+
+def hand_out(outs):
+    return pl.pallas_call(
+        hand_on,
+        out_shape=tuple(jax.ShapeDtypeStruct(o.shape, o.dtype) for o in outs),
+        in_specs=[pl.BlockSpec(memory_space=pltpu.VMEM)] * 2,
+        out_specs=[pl.BlockSpec(memory_space=pl.ANY)] * 2,
+        scratch_shapes=[pltpu.SemaphoreType.DMA((2,))],
+    )(*(pltpu.with_memory_space_constraint(o, pltpu.VMEM) for o in outs))
 
 
 def shards(
@@ -863,8 +967,8 @@
     outs = pl.pallas_call(
         body,
         out_shape=(
-            jax.ShapeDtypeStruct((length, out_w), BF16),
-            jax.ShapeDtypeStruct((length, out_w), BF16),
+            pltpu.VMEM((length, out_w), BF16),
+            pltpu.VMEM((length, out_w), BF16),
         ),
         in_specs=specs,
         out_specs=(vmem, vmem),
@@ -873,12 +977,7 @@
             collective_id=0, has_side_effects=True, vmem_limit_bytes=60 * 1024 * 1024
         ),
     )(*operands)
-    return pl.pallas_call(
-        hand_on,
-        out_shape=tuple(jax.ShapeDtypeStruct(o.shape, o.dtype) for o in outs),
-        in_specs=(vmem, vmem),
-        out_specs=(vmem, vmem),
-    )(*outs)
+    return hand_out(outs)
 
 
 def solution(mesh):

time: 60.7 us -> 56.8 us (0.936); the launches traced: 60.5 us -> 55.8 us
  Pallas kernels: 59.9 us -> 55 us
    pallas_call x2, Pallas kernels: 59.9 us -> 55 us  [the longest x1 54.2 us: shards(): pl.pallas_call(body, out_shape=(pltpu.VMEM((length, out_w), BF16), pltpu....]
where the time goes in v2:
time: 56.8 us; the launch traced here: 55.8 us
  Pallas kernels  55 us (97%)
  between operations  0.8 us (1%)
    pallas_call x1, Pallas kernels, shards(): pl.pallas_call(body, out_shape=(pltpu.VMEM((length, out_w), BF16), pltpu....  54.2 us

profile of v2, /device:TPU:0, one launch (start us, length us, event | category | flops | bytes accessed | tf_op | source)
XLA Modules:
  0.0 55.8 jit_solution(17037507163352472150)
XLA Ops:
  0.6 54.2 %shard_map.149 = (bf16[256,512]{1,0:T(8,128)(2,1)S(1)}, bf16[256,512]{1,0:T(8,128)(2,1)S(1)}) custom-call(bf16[256,256]{1,0:T(8,128)(2,1)} %q_ref.1, bf16[256,128]{1,0:T(8,128)(2,1)} %k_ref.1, bf16[256,128]{1,0:T(8,128)(2,1)} %v_ref.1, f32[1,64]{1,0:T(1,128)} %bitcast.18, f32[1,64]{1,0:T(1,128)} %bitcast.19, f32[8,1,256]{2,1,0:T(1,128)} %bitcast.15, ...), custom_call_target="tpu_custom_call" | custom-call | tf_op jit(solution)/shard_map/pallas_call | solution.py:967
  54.8 0.8 %shard_map.150 = (bf16[256,512]{1,0:T(8,128)(2,1)}, bf16[256,512]{1,0:T(8,128)(2,1)}) custom-call(bf16[256,512]{1,0:T(8,128)(2,1)S(1)} %get-tuple-element.4.a_ref, bf16[256,512]{1,0:T(8,128)(2,1)S(1)} %get-tuple-element.5.b_ref), custom_call_target="tpu_custom_call" | custom-call | tf_op jit(solution)/shard_map/pallas_call | solution.py:896

commit v3 on v2

--- a/solution.py
+++ b/solution.py
@@ -442,6 +442,8 @@
 NEEDS = {FORWARD: 0, SIDE: 1, CORNER: 2}
 NEAR = (0, 2, 4, 6)
 FAR = (1, 3, 5, 7)
+FIRST = NEAR[:3]
+SECOND = NEAR[3:] + FAR
 
 
 class Relay:
@@ -490,11 +492,8 @@
         if block in FAR:
             self.wait(3)
         elif block:
-            for i in (0, 1, 2):
+            for i in (0, 1, 2) if block in SECOND else (0, 1):
                 self.wait(i)
-
-    def drain(self):
-        self.whole(len(FAR) + 3, 0).wait_send()
 
 
 def line_kernel(
@@ -542,10 +541,10 @@
         )
 
     def x_copy(d):
-        return ep_copy(xo.at[d], xb.at[d, 0], d, z_send.at[0], z_recv.at[0, d])
+        return ep_copy(xo.at[d], xb.at[d, 0], d, z_send.at[0], z_recv.at[0, d - 1])
 
     def r_copy(d):
-        return ep_copy(ob.at[d], rb.at[d], d, z_send.at[1], z_recv.at[1, d])
+        return ep_copy(ob.at[d], rb.at[d], d, z_send.at[1], z_recv.at[1, d - 1])
 
     def kv_copy(i):
         d, block = ((1, 0), (2, 0), (1, 2))[i]
@@ -555,15 +554,17 @@
 
     def fresh():
         live.fetched = set()
+        live.partial = {}
         live.xt = [
-            Relay(f"x{d}", xb.at[d], t_send.at[0, d], t_recv.at[0, d], tp) for d in range(n_ep)
+            Relay(f"x{d}", xb.at[d], t_send.at[0], t_recv.at[d], tp) for d in range(n_ep)
         ]
         live.ht = [
-            Relay(f"h{d}", hb.at[d], t_send.at[1, d], t_recv.at[1, d], tp) for d in range(n_ep)
+            Relay(f"h{d}", hb.at[d], t_send.at[1], t_recv.at[n_ep + d], tp) for d in range(n_ep)
         ]
         live.mt = [
             Relay(
-                f"m{k}", mb.at[:, pl.ds(k * half, half)], t_send.at[2, k], t_recv.at[2, k], tp
+                f"m{k}", mb.at[:, pl.ds(k * half, half)],
+                t_send.at[2], t_recv.at[2 * n_ep + k], tp,
             )
             for k in range(2)
         ]
@@ -621,28 +622,36 @@
         with jax.named_scope(f"wxz_{d}"):
             x_copy(d).wait_recv()
 
-    def hidden(d):
-        total = jnp.zeros((cap, 2 * ffw), F32)
-        squares = jnp.zeros((cap, 1), F32)
-        for m in NEAR + FAR:
+    def hidden(d, blocks=NEAR + FAR, last=True):
+        total, squares = live.partial.pop(("x", d), (None, None))
+        for m in blocks:
             live.xt[d].ready(m)
             weights(0)
             weights(1)
             block = xb[d, m].astype(F32)
-            squares += jnp.sum(block * block, axis=1, keepdims=True)
+            square = jnp.sum(block * block, axis=1, keepdims=True)
             scaled = (block * xg_ref[tp ^ m]).astype(BF16)
-            total += jnp.dot(scaled, wgu[tp ^ m], preferred_element_type=F32)
+            product = jnp.dot(scaled, wgu[tp ^ m], preferred_element_type=F32)
+            total = product if total is None else total + product
+            squares = square if squares is None else squares + square
+        if not last:
+            live.partial["x", d] = total, squares
+            return
         stat = lax.rsqrt(squares / xg_ref.shape[0] / xg_ref.shape[2] + EPS)
         gate = total[:, :ffw] * stat
         up = total[:, ffw:] * stat
         hb[d, 0] = (gate / (1.0 + jnp.exp(-gate)) * up).astype(BF16)
 
-    def down(d):
-        total = jnp.zeros((ob.shape[1], ob.shape[2]), F32)
-        for m in NEAR + FAR:
+    def down(d, blocks=NEAR + FAR, last=True):
+        total = live.partial.pop(("h", d), None)
+        for m in blocks:
             live.ht[d].ready(m)
             weights(2)
-            total += jnp.dot(hb[d, m], wd[tp ^ m], preferred_element_type=F32)
+            product = jnp.dot(hb[d, m], wd[tp ^ m], preferred_element_type=F32)
+            total = product if total is None else total + product
+        if not last:
+            live.partial["h", d] = total
+            return
         ob[d] = total.astype(BF16)
         if d:
             r_copy(d).start()
@@ -715,8 +724,17 @@
         with jax.named_scope("S_" + name):
             f(*args, **kwargs)
 
+    def on_core(core, name, f, *args):
+        @pl.when(tp % 2 == core)
+        def _():
+            step(name, f, *args)
+
+    def pick_x(d):
+        xo[d] = picked_rows(d)
+
     def send_x(d):
-        xo[d] = picked_rows(d)
+        if d == 3:
+            pick_x(d)
         x_copy(d).start()
 
     def finish():
@@ -724,19 +742,26 @@
             for i, buf in enumerate((xo, rb, kv)):
                 part = buf.at[pl.ds(0, n_ep - 1)]
                 ep_copy(part, part, 1, z_send.at[i], z_recv.at[i, 0]).wait_send()
-            for gather in live.xt + live.ht + live.mt:
-                gather.drain()
+            sent = pl.ds(0, n_tp - 1)
+            for i, part in enumerate((xb.at[:, sent], hb.at[:, sent], mb.at[sent])):
+                pltpu.make_async_remote_copy(
+                    src_ref=part, dst_ref=part, send_sem=t_send.at[i], recv_sem=t_recv.at[0, 0],
+                    device_id={"tp": tp ^ 1}, device_id_type=MESH,
+                ).wait_send()
 
     for copy in local:
         copy.start()
     xb[0, 0] = picked_rows(0)
+    pick_x(2)
+    pick_x(1)
     with jax.named_scope("S_barrier"):
         pl.semaphore_wait(barrier, n_ep + n_tp - 2)
     fresh()
-    step("X0own", live.xt[0].issue, OWN)
     step("sx2", send_x, 2)
     step("sx1", send_x, 1)
+    step("X0lead", live.xt[0].issue, LEAD)
     step("keys", own_keys)
+    step("X0rest", live.xt[0].issue, REST)
     step("columns", columns)
 
     @pl.when(inner == 1)
@@ -781,32 +806,35 @@
         step("H3own", live.ht[3].issue, OWN)
         step("H1side", live.ht[1].issue, SIDE)
         step("att01", attention, 0, 1)
-        step("M0own", live.mt[0].issue, OWN)
+        on_core(0, "M0own", live.mt[0].issue, OWN)
         step("H1cor", live.ht[1].issue, CORNER)
         step("att10", attention, 1, 0)
+        on_core(1, "M0own", live.mt[0].issue, OWN)
         step("H3fwd", live.ht[3].issue, FORWARD)
-        step("H0own", live.ht[0].issue, OWN)
         step("down1", down, 1)
         step("att11", attention, 1, 1)
+        step("H0own", live.ht[0].issue, OWN)
         step("M0fwd", live.mt[0].issue, FORWARD)
         step("M1own", live.mt[1].issue, OWN)
         step("H3side", live.ht[3].issue, SIDE)
+        step("downa3", down, 3, FIRST, False)
         step("H3cor", live.ht[3].issue, CORNER)
         step("M0side", live.mt[0].issue, SIDE)
-        step("down3", down, 3)
+        step("downb3", down, 3, SECOND)
+        step("comb2F", combine, 2, first=True)
         step("H0fwd", live.ht[0].issue, FORWARD)
         step("M0cor", live.mt[0].issue, CORNER)
         step("M1fwd", live.mt[1].issue, FORWARD)
         step("H0side", live.ht[0].issue, SIDE)
+        step("downa0", down, 0, FIRST, False)
         step("H0cor", live.ht[0].issue, CORNER)
+        step("M1side", live.mt[1].issue, SIDE)
         step("project0", project, 0)
-        step("M1side", live.mt[1].issue, SIDE)
-        step("down0", down, 0)
-        step("comb0F", combine, 0, first=True)
         step("M1cor", live.mt[1].issue, CORNER)
-        step("comb2", combine, 2)
+        step("downb0", down, 0, SECOND)
+        step("comb0", combine, 0)
+        step("project1", project, 1)
         step("comb1", combine, 1)
-        step("project1", project, 1)
         step("comb3L", combine, 3, last=True)
         finish()
 
@@ -835,48 +863,53 @@
         step("X2cor", live.xt[2].issue, CORNER)
         step("X3fwd", live.xt[3].issue, FORWARD)
         step("hid2", hidden, 2)
-        step("H2own", live.ht[2].issue, OWN)
-        step("H1own", live.ht[1].issue, OWN)
+        on_core(0, "H2own", live.ht[2].issue, OWN)
+        on_core(0, "H1own", live.ht[1].issue, OWN)
         step("X3side", live.xt[3].issue, SIDE)
+        step("hida3", hidden, 3, FIRST, False)
         step("keyson", keys_on)
         step("X3cor", live.xt[3].issue, CORNER)
+        on_core(1, "H2own", live.ht[2].issue, OWN)
+        on_core(1, "H1own", live.ht[1].issue, OWN)
         step("H2fwd", live.ht[2].issue, FORWARD)
-        step("hid3", hidden, 3)
+        step("hidb3", hidden, 3, SECOND)
         step("H3own", live.ht[3].issue, OWN)
         step("H2side", live.ht[2].issue, SIDE)
-        step("H1fwd", live.ht[1].issue, FORWARD)
         step("wkv", keys_ready)
         step("att00", attention, 0, 0)
         step("H2cor", live.ht[2].issue, CORNER)
+        step("H3fwd", live.ht[3].issue, FORWARD)
+        step("H1fwd", live.ht[1].issue, FORWARD)
         step("down2", down, 2)
         step("H1side", live.ht[1].issue, SIDE)
-        step("H3fwd", live.ht[3].issue, FORWARD)
         step("att01", attention, 0, 1)
         step("M0own", live.mt[0].issue, OWN)
+        step("H3side", live.ht[3].issue, SIDE)
+        step("att10", attention, 1, 0)
         step("H0own", live.ht[0].issue, OWN)
+        step("downa3", down, 3, FIRST, False)
+        step("H3cor", live.ht[3].issue, CORNER)
+        step("downb3", down, 3, SECOND)
         step("H1cor", live.ht[1].issue, CORNER)
-        step("att10", attention, 1, 0)
-        step("H3side", live.ht[3].issue, SIDE)
         step("att11", attention, 1, 1)
         step("M1own", live.mt[1].issue, OWN)
-        step("H3cor", live.ht[3].issue, CORNER)
-        step("down3", down, 3)
         step("M0fwd", live.mt[0].issue, FORWARD)
         step("down1", down, 1)
         step("M0side", live.mt[0].issue, SIDE)
         step("H0fwd", live.ht[0].issue, FORWARD)
+        step("comb2F", combine, 2, first=True)
         step("M1fwd", live.mt[1].issue, FORWARD)
         step("M0cor", live.mt[0].issue, CORNER)
         step("H0side", live.ht[0].issue, SIDE)
+        step("downa0", down, 0, FIRST, False)
         step("H0cor", live.ht[0].issue, CORNER)
+        step("M1side", live.mt[1].issue, SIDE)
         step("project0", project, 0)
-        step("M1side", live.mt[1].issue, SIDE)
-        step("down0", down, 0)
-        step("comb0F", combine, 0, first=True)
+        step("M1cor", live.mt[1].issue, CORNER)
+        step("downb0", down, 0, SECOND)
+        step("comb0", combine, 0)
+        step("project1", project, 1)
         step("comb1", combine, 1)
-        step("M1cor", live.mt[1].issue, CORNER)
-        step("comb2", combine, 2)
-        step("project1", project, 1)
         step("comb3L", combine, 3, last=True)
         finish()
 
@@ -957,7 +990,7 @@
         body = functools.partial(line_kernel, n_ep, n_tp, cap)
         scratch = tables_at + blocks_at + [pltpu.VMEM((n_ep, length, 2 * kw), BF16)]
         scratch += results_at + [pltpu.VMEM((2, length, out_w), F32)] + weights_at
-        scratch += [dma((4,)), dma((3,)), dma((3, n_ep)), dma((3, n_ep)), dma((3, n_ep, 4))]
+        scratch += [dma((4,)), dma((3,)), dma((3, n_ep - 1)), dma((3,)), dma((2 * n_ep + 2, 4))]
     else:
         body = functools.partial(kernel, n_ep, n_tp, cap, plan)
         scratch = tables_at + blocks_at + [pltpu.VMEM((n_ep, length, kw), BF16)] * 2

time: 56.8 us -> 55.7 us (0.981); the launches traced: 55.8 us -> 55.4 us
  no operation moved by 1% of the time
where the time goes in v3:
time: 55.7 us; the launch traced here: 55.4 us
  Pallas kernels  54.6 us (98%)
  between operations  0.8 us (1%)
    pallas_call x1, Pallas kernels, shards(): pl.pallas_call(body, out_shape=(pltpu.VMEM((length, out_w), BF16), pltpu....  53.7 us

profile of v3, /device:TPU:0, one launch (start us, length us, event | category | flops | bytes accessed | tf_op | source)
XLA Modules:
  0.0 55.4 jit_solution(1963059404096199049)
XLA Ops:
  0.6 53.7 %shard_map.149 = (bf16[256,512]{1,0:T(8,128)(2,1)S(1)}, bf16[256,512]{1,0:T(8,128)(2,1)S(1)}) custom-call(bf16[256,256]{1,0:T(8,128)(2,1)} %q_ref.1, bf16[256,128]{1,0:T(8,128)(2,1)} %k_ref.1, bf16[256,128]{1,0:T(8,128)(2,1)} %v_ref.1, f32[1,64]{1,0:T(1,128)} %bitcast.18, f32[1,64]{1,0:T(1,128)} %bitcast.19, f32[8,1,256]{2,1,0:T(1,128)} %bitcast.15, ...), custom_call_target="tpu_custom_call" | custom-call | tf_op jit(solution)/shard_map/pallas_call | solution.py:1000
  54.4 0.8 %shard_map.150 = (bf16[256,512]{1,0:T(8,128)(2,1)}, bf16[256,512]{1,0:T(8,128)(2,1)}) custom-call(bf16[256,512]{1,0:T(8,128)(2,1)S(1)} %get-tuple-element.4.a_ref, bf16[256,512]{1,0:T(8,128)(2,1)S(1)} %get-tuple-element.5.b_ref), custom_call_target="tpu_custom_call" | custom-call | tf_op jit(solution)/shard_map/pallas_call | solution.py:929

commit v4 on v3

--- a/solution.py
+++ b/solution.py
@@ -703,15 +703,17 @@
         places["weight"] = [column[:, 2 + k : 3 + k] for k in range(2)]
 
     def combine(d, first=False, last=False):
+        index = (ep ^ d) * cap + iota((length, cap), 1)
+        choose = [
+            jnp.where(places["slot"][k] == index, 1.0, 0.0).astype(BF16) for k in range(2)
+        ]
         if d:
             with jax.named_scope(f"wr_{d}"):
                 r_copy(d).wait_recv()
         back = rb[d] if d else ob[0]
-        index = (ep ^ d) * cap + iota((length, cap), 1)
         total = []
         for k in range(2):
-            choose = jnp.where(places["slot"][k] == index, 1.0, 0.0).astype(BF16)
-            found = jnp.dot(choose, back, preferred_element_type=F32)
+            found = jnp.dot(choose[k], back, preferred_element_type=F32)
             total.append(found if first else ct[k] + found)
         if last:
             weight = places["weight"]

time: 55.7 us -> 55.7 us (level)
  no operation moved by 1% of the time
where the time goes in v4:
time: 55.7 us; the launch traced here: 55.4 us
  Pallas kernels  54.6 us (98%)
  between operations  0.8 us (1%)
    pallas_call x1, Pallas kernels, shards(): pl.pallas_call(body, out_shape=(pltpu.VMEM((length, out_w), BF16), pltpu....  53.8 us

profile of v4, /device:TPU:0, one launch (start us, length us, event | category | flops | bytes accessed | tf_op | source)
XLA Modules:
  0.0 55.4 jit_solution(380061831969767047)
XLA Ops:
  0.6 53.8 %shard_map.149 = (bf16[256,512]{1,0:T(8,128)(2,1)S(1)}, bf16[256,512]{1,0:T(8,128)(2,1)S(1)}) custom-call(bf16[256,256]{1,0:T(8,128)(2,1)} %q_ref.1, bf16[256,128]{1,0:T(8,128)(2,1)} %k_ref.1, bf16[256,128]{1,0:T(8,128)(2,1)} %v_ref.1, f32[1,64]{1,0:T(1,128)} %bitcast.18, f32[1,64]{1,0:T(1,128)} %bitcast.19, f32[8,1,256]{2,1,0:T(1,128)} %bitcast.15, ...), custom_call_target="tpu_custom_call" | custom-call | tf_op jit(solution)/shard_map/pallas_call | solution.py:1002
  54.4 0.8 %shard_map.150 = (bf16[256,512]{1,0:T(8,128)(2,1)}, bf16[256,512]{1,0:T(8,128)(2,1)}) custom-call(bf16[256,512]{1,0:T(8,128)(2,1)S(1)} %get-tuple-element.4.a_ref, bf16[256,512]{1,0:T(8,128)(2,1)S(1)} %get-tuple-element.5.b_ref), custom_call_target="tpu_custom_call" | custom-call | tf_op jit(solution)/shard_map/pallas_call | solution.py:931
